TPU v7x, 32 devices: a whole 2x2x4 slice. The times are simulated.
32 devices in a mesh: grp: 2 (over y), sp: 4 (over z), tp: 4 (over x, core).
Axes of the slice: x: 2, y: 2, z: 4, core: 2. Of those that a mesh axis runs over, the one named last changes fastest.
Arguments:
- tokens: bfloat16 [4096, 2048], P(('grp', 'sp', 'tp')), parts along dimension 0, may hold values from -6 to 6
- norm_gain: bfloat16 [2048], replicated, may hold values from 0.099609375 to 1.8984375
- conv_outer_weight: bfloat16 [2048, 1024], P('sp', 'tp'), may hold values from -0.125 to 0.125
- conv_inner_weight: bfloat16 [2048, 1024], P('sp', 'tp'), may hold values from -0.125 to 0.125
- conv_input_weight: bfloat16 [2048, 1024], P('sp', 'tp'), may hold values from -0.125 to 0.125
- query_matrix: bfloat16 [2048, 1024], P('sp', 'tp'), may hold values from -0.125 to 0.125
- key_weight: bfloat16 [2048, 1024], P('sp', 'tp'), may hold values from -0.125 to 0.125
- value_weight: bfloat16 [2048, 1024], P('sp', 'tp'), may hold values from -0.125 to 0.125
- gate_weight: bfloat16 [2048, 1024], P('sp', 'tp'), may hold values from -0.125 to 0.125
- conv_taps: bfloat16 [3, 1024], P(None, 'tp'), may hold values from -3.5 to 3.5
- conv_out_weight: bfloat16 [1024, 2048], P('tp', 'sp'), may hold values from -0.125 to 0.125
- ret_out_weight: bfloat16 [1024, 2048], P('tp', 'sp'), may hold values from -0.125 to 0.125
- log_decay: float32 [4096, 8], P(('grp', 'sp'), 'tp'), parts along dimension 0, may hold values from -0.75 to 0
Outputs:
- mixed: bfloat16 [4096, 2048], P(('grp', 'sp', 'tp')), parts along dimension 0
There are 2 independent parts, one for each index of `grp`. A program takes and returns all parts, laid end to end along the dimension named above; an argument that names none is the same for every part. Nothing has to cross between parts.
All inputs are finite; a program needn't handle non-finite values.
Results may differ from a plain program's by a relative error of at most 0.025.
Values may be sent and summed in bfloat16 or wider, within the bound.
A program may use at most 64 MiB of HBM per device.

v0:
```python
import jax
import jax.numpy as jnp
from jax import lax
from jax.sharding import PartitionSpec as P

HEAD = 128
CONV_K = 3
BLOCK = 128
EPSILON = 1e-06
ROTARY_BASE = 10000.0
HIGHEST_PRECISION = lax.Precision.HIGHEST


def prefix_2(x, axis, join, neutral):
    place = lax.axis_index(axis)
    gathered = jax.tree.map(
        lambda a, kind: lax.all_gather(a.astype(kind), axis), x, (jnp.bfloat16, jnp.bfloat16)
    )
    state = jax.tree.map(lambda a, e: jnp.zeros_like(a) + jnp.asarray(e, a.dtype), x, neutral)

    def one(turn, state):
        return join(
            state,
            jax.tree.map(
                lambda a, own: lax.dynamic_index_in_dim(a, turn, 0, False).astype(own.dtype),
                gathered,
                x,
            ),
        )

    return lax.fori_loop(0, place, one, state)


def shifted(x, axis, by):
    count = lax.axis_size(axis)
    pairs = [(i, i + by) for i in range(count) if 0 <= i + by < count]
    return lax.ppermute(x, axis, pairs)


def rotate(head_data, positions):
    half_width = head_data.shape[-1] // 2
    inv_freq = ROTARY_BASE ** (-jnp.arange(half_width, dtype=jnp.float32) / half_width)
    angles = positions[:, None] * inv_freq[None, :]
    cosine = jnp.cos(angles)[:, None, :]
    sine_part = jnp.sin(angles)[:, None, :]
    first_half = head_data[..., :half_width]
    second_half = head_data[..., half_width:]
    return jnp.concatenate(
        [
            first_half * cosine - second_half * sine_part,
            second_half * cosine + first_half * sine_part,
        ],
        axis=-1,
    )


def head_norm(head_data):
    return head_data * lax.rsqrt(jnp.mean(head_data * head_data, axis=-1, keepdims=True) + EPSILON)


def combine_states(earlier, later):
    return (earlier[0] * later[0], later[0][:, None, None] * earlier[1] + later[1])


def body(
    tokens,
    norm_gain,
    conv_outer_weight,
    conv_inner_weight,
    conv_input_weight,
    query_matrix,
    key_weight,
    value_weight,
    gate_weight,
    conv_taps,
    conv_out_weight,
    ret_out_weight,
    log_decay,
):
    values32 = tokens.astype(jnp.float32)
    normed = (
        values32
        * lax.rsqrt(jnp.mean(values32 * values32, axis=-1, keepdims=True) + EPSILON)
        * norm_gain.astype(jnp.float32)
    ).astype(jnp.bfloat16)
    gathered = lax.all_gather(normed, "tp", axis=0, tiled=True)
    row_total = gathered.shape[0]
    whole = (
        lax.all_gather(conv_outer_weight, "sp", axis=0, tiled=True),
        lax.all_gather(conv_inner_weight, "sp", axis=0, tiled=True),
        lax.all_gather(conv_input_weight, "sp", axis=0, tiled=True),
        lax.all_gather(query_matrix, "sp", axis=0, tiled=True),
        lax.all_gather(key_weight, "sp", axis=0, tiled=True),
        lax.all_gather(value_weight, "sp", axis=0, tiled=True),
        lax.all_gather(gate_weight, "sp", axis=0, tiled=True),
    )
    projected = tuple(
        (
            jnp.dot(gathered, weight, preferred_element_type=jnp.float32).astype(jnp.bfloat16)
            for weight in whole
        )
    )
    conv_outer, conv_inner, conv_input, query_proj, key_proj, value_proj, gate_proj = projected
    heads_here = query_proj.shape[1] // HEAD
    offset = (lax.axis_index("sp") * row_total).astype(jnp.float32)
    positions = offset + jnp.arange(row_total, dtype=jnp.float32)
    head_shape = (row_total, heads_here, HEAD)
    queries = rotate(query_proj.astype(jnp.float32).reshape(head_shape), positions)
    keys_rot = rotate(key_proj.astype(jnp.float32).reshape(head_shape), positions) * HEAD ** (-0.5)
    head_values = value_proj.astype(jnp.float32).reshape(head_shape)
    block_count = row_total // BLOCK
    block_shape = (block_count, BLOCK, heads_here, HEAD)
    query_blocks = queries.reshape(block_shape)
    key_blocks = keys_rot.reshape(block_shape)
    value_blocks = head_values.reshape(block_shape)
    log_blocks = log_decay.reshape(block_count, BLOCK, heads_here)
    offsets = jnp.arange(BLOCK, dtype=jnp.int32)
    causal_mask = offsets[:, None] >= offsets[None, :]
    lower_ones = causal_mask.astype(jnp.float32)
    cumulative = jnp.einsum("ij,njh->nih", lower_ones, log_blocks, precision=HIGHEST_PRECISION)
    block_end = cumulative[:, -1, :]
    mixed_in = conv_inner.astype(jnp.float32) * conv_input.astype(jnp.float32)
    rim = shifted(mixed_in[row_total - (CONV_K - 1) :], "sp", 1)
    extended = jnp.concatenate([rim, mixed_in], axis=0)
    taps = conv_taps.astype(jnp.float32)
    conv_out = jnp.zeros(mixed_in.shape, jnp.float32)
    for tap_index in range(CONV_K):
        conv_out = conv_out + taps[tap_index][None, :] * extended[tap_index : tap_index + row_total]
    conv_branch = (conv_outer.astype(jnp.float32) * conv_out).astype(jnp.bfloat16)
    weights = jnp.exp(block_end[:, None, :] - cumulative)
    increments = jnp.einsum(
        "njh,njhd,njhe->nhde", weights, key_blocks, value_blocks, precision=HIGHEST_PRECISION
    )

    def carry_on(carried, pieces):
        block_decay, increment = pieces
        return (block_decay[:, None, None] * carried + increment, carried)

    start_state = jnp.zeros((heads_here, HEAD, HEAD), jnp.float32)
    local_end, local_before = lax.scan(carry_on, start_state, (jnp.exp(block_end), increments))
    device_decay = jnp.exp(jnp.sum(block_end, axis=0))
    incoming = prefix_2(
        (device_decay, local_end),
        "sp",
        combine_states,
        (jnp.ones_like(device_decay), jnp.zeros_like(local_end)),
    )
    local_before, incoming_state = (local_before, incoming[1])
    spread = cumulative[:, :, None, :] - cumulative[:, None, :, :]
    grid_mask = causal_mask[None, :, :, None]
    decay_grid = jnp.where(grid_mask, jnp.exp(jnp.where(grid_mask, spread, 0.0)), 0.0)
    scores = (
        jnp.einsum("nihd,njhd->nijh", query_blocks, key_blocks, precision=HIGHEST_PRECISION)
        * decay_grid
    )
    within = jnp.einsum("nijh,njhe->nihe", scores, value_blocks, precision=HIGHEST_PRECISION)
    prefix = jnp.exp(jnp.cumsum(block_end, axis=0) - block_end)
    before = local_before + prefix[:, :, None, None] * incoming_state[None]
    across = jnp.einsum("nihd,nhde->nihe", query_blocks, before, precision=HIGHEST_PRECISION)
    across = across * jnp.exp(cumulative)[..., None]
    retained = (within + across).reshape(head_shape)
    ret_branch = (
        head_norm(retained).reshape(row_total, heads_here * HEAD)
        * jax.nn.silu(gate_proj.astype(jnp.float32))
    ).astype(jnp.bfloat16)
    conv_rows_weight, ret_rows_weight = (
        lax.all_gather(conv_out_weight, "sp", axis=1, tiled=True),
        lax.all_gather(ret_out_weight, "sp", axis=1, tiled=True),
    )
    return lax.psum_scatter(
        (
            jnp.dot(conv_branch, conv_rows_weight, preferred_element_type=jnp.float32)
            + jnp.dot(ret_branch, ret_rows_weight, preferred_element_type=jnp.float32)
        ).astype(jnp.bfloat16),
        "tp",
        scatter_dimension=0,
        tiled=True,
    )


def solution(mesh):
    placed = (
        P(("grp", "sp", "tp"), None),
        P(),
        P("sp", "tp"),
        P("sp", "tp"),
        P("sp", "tp"),
        P("sp", "tp"),
        P("sp", "tp"),
        P("sp", "tp"),
        P("sp", "tp"),
        P(None, "tp"),
        P("tp", "sp"),
        P("tp", "sp"),
        P(("grp", "sp"), "tp"),
    )
    return jax.shard_map(
        body, mesh=mesh, in_specs=placed, out_specs=P(("grp", "sp", "tp"), None), check_vma=False
    )
```

profile of v0, /device:TPU:0, one launch (start us, length us, event | category | flops | bytes accessed | tf_op | source)
XLA Modules:
  0.0 343.9 jit_solution(5092971589011308150)
XLA Ops:
  6.5 0.7 all-gather.25.cloned.1.call-update
  7.3 0.7 convert_element_type.96
  8.0 1.3 fusion.9
  9.3 2.0 fusion.11
  11.4 0.7 all-gather.27.cloned.1.call-update
  13.9 0.7 all-gather.15.cloned.1.call-update
  14.6 0.7 all-gather.21.cloned.1.call-update
  15.4 0.7 all-gather.29.cloned.1.call-update
  20.9 14.0 %all-reduce = bf16[8]{0:T(256)(128)(2,1)S(1)} all-reduce(bf16[8]{0:T(256)(128)(2,1)S(1)} %dynamic-update-slice), channel_id=2, replica_groups=mesh['grp'=2,'sp'=4,'tp'=4] {'sp'}, use_global_device_ids=true, to_apply=%add | all-reduce | flops 8 | bytes 32
  37.4 1.8 multiply_cosine_fusion
  39.2 0.7 all-gather.25.cloned.1.call-done
  39.9 23.6 %all-gather.13.cloned.1.call-done = bf16[512,2048]{1,0:T(8,128)(2,1)} async-done(((bf16[128,2048]{1,0:T(8,128)(2,1)}), bf16[512,2048]{1,0:T(8,128)(2,1)}) %all-gather.13.cloned.1.call-update) | async-done | bytes 2097168 | tf_op jit(solution)/shard_map/all_gather | solution.py:86
  63.5 2.6 convolution_convert_fusion.2
  66.2 1.0 copy.95
  67.2 1.0 copy.96
  68.2 24.9 %all-gather.27.cloned.1.call-done = bf16[2048,256]{1,0:T(8,128)(2,1)} async-done(((bf16[512,256]{1,0:T(8,128)(2,1)}), bf16[2048,256]{1,0:T(8,128)(2,1)}) %all-gather.27.cloned.1.call-update) | async-done | bytes 1048592 | tf_op jit(solution)/shard_map/all_gather | solution.py:92
  93.1 2.0 convolution_convert_fusion.1
  95.1 1.0 copy.97
  96.1 1.0 copy.98
  97.1 24.8 %all-gather.23.cloned.1.call-done = bf16[2048,256]{1,0:T(8,128)(2,1)} async-done(((bf16[512,256]{1,0:T(8,128)(2,1)}), bf16[2048,256]{1,0:T(8,128)(2,1)}) %all-gather.23.cloned.1.call-update) | async-done | bytes 1048592 | tf_op jit(solution)/shard_map/all_gather | solution.py:94
  121.9 1.9 convolution_convert_fusion.3
  123.9 2.9 multiply_subtract_fusion
  126.8 1.7 fusion.23
  128.5 9.4 %while.26 = (s32[]{:T(128)}, f32[2,128,128]{2,1,0:T(8,128)S(1)}, f32[4,2,128,128]{3,2,1,0:T(8,128)}, f32[4,2]{1,0:T(4,128)}, f32[4,2,128,128]{3,2,1,0:T(8,128)}, /*index=5*/s32[]{:T(128)}, s32[]{:T(128)}) while((s32[]{:T(128)}, f32[2,128,128]{2,1,0:T(8,128)S(1)}, f32[4,2,128,128]{3,2,1,0:T(8,128)}, f32[4,2]{1,0:T(4,128)}, ...), condition=%wide.region_2.3_spmd.clone, body=%wide.region_1.2_spmd.clone.sunk | while | flops 131075 | bytes 655992 | solution.py:140
  129.1 0.7 fusion.69
  129.8 1.0 bitcast_add_fusion.2
  131.5 0.7 fusion.69
  132.1 1.0 bitcast_add_fusion.2
  133.1 0.7 bitcast_dynamic-update-slice_fusion.2
  133.8 0.7 fusion.69
  134.5 1.0 bitcast_add_fusion.2
  135.5 0.7 bitcast_dynamic-update-slice_fusion.2
  136.8 1.0 bitcast_add_fusion.2
  137.9 17.1 %all-gather.1 = bf16[8,128,128]{2,1,0:T(8,128)(2,1)} all-gather(bf16[2,128,128]{2,1,0:T(8,128)(2,1)S(1)} %convert_element_type.112), channel_id=3, replica_groups=mesh['grp'=2,'sp'=4,'tp'=4] {'sp'}, dimensions={0}, use_global_device_ids=true | all-gather | bytes 327680 | tf_op jit(solution)/shard_map/all_gather | solution.py:17
  155.0 2.7 fusion.7
  157.7 26.0 %all-gather.17.cloned.1.call-done = bf16[2048,256]{1,0:T(8,128)(2,1)} async-done(((bf16[512,256]{1,0:T(8,128)(2,1)}), bf16[2048,256]{1,0:T(8,128)(2,1)}) %all-gather.17.cloned.1.call-update) | async-done | bytes 1048592 | tf_op jit(solution)/shard_map/all_gather | solution.py:90
  183.7 2.2 fusion.6
  186.6 3.9 %collective-permute-start = (f32[2,256]{1,0:T(2,128)}, f32[2,256]{1,0:T(2,128)}, u32[]{:S(2)}, u32[]{:S(2)}) collective-permute-start(f32[2,256]{1,0:T(2,128)} %slice.45), channel_id=1, source_target_pairs={{0,4},{4,8},{8,12},{1,5},{5,9},{9,13},{2,6},{6,10},{10,14},{3,7},{... | collective-permute-start | bytes 6152 | tf_op jit(solution)/shard_map/ppermute | solution.py:37
  190.7 1.3 fusion.3
  192.5 1.9 multiply_reduce_fusion
  194.5 1.3 copy.85
  195.8 16.9 %all-gather.15.cloned.1.call-done = bf16[2048,256]{1,0:T(8,128)(2,1)} async-done(((bf16[512,256]{1,0:T(8,128)(2,1)}), bf16[2048,256]{1,0:T(8,128)(2,1)}) %all-gather.15.cloned.1.call-update) | async-done | bytes 1048592 | tf_op jit(solution)/shard_map/all_gather | solution.py:89
  212.7 29.0 %all-gather.21.cloned.1.call-done = bf16[256,2048]{1,0:T(8,128)(2,1)} async-done(((bf16[256,512]{1,0:T(8,128)(2,1)}), bf16[256,2048]{1,0:T(8,128)(2,1)}) %all-gather.21.cloned.1.call-update) | async-done | bytes 1048592 | tf_op jit(solution)/shard_map/all_gather | solution.py:167
  241.7 5.8 %fusion.30 = f32[512,2048]{1,0:T(8,128)} fusion(bf16[256,2048]{1,0:T(8,128)(2,1)} %all-gather.21.cloned.1.call-done, f32[2,256]{1,0:T(2,128)} %collective-permute-done, f32[512,256]{1,0:T(8,128)S(1)} %copy-done.2, bf16[512,2048]{1,0:T(8,128)(2,1)S(1)} %copy-done, bf16[2048,256]{1,0:T(8,128)(2,1)} %all-gather.15.cloned.1.call-done, f32[256]{0:T(256)S(1)} %bitcast.101, ...), kind=kOutput, calls=%fused_computation.62 | convolution fusion | flops 1075183616 | bytes 8918016 | tf_op jit(solution)/shard_map/dot_general | solution.py:172
  247.5 23.1 %all-gather.29.cloned.1.call-done = bf16[2048,256]{1,0:T(8,128)(2,1)} async-done(((bf16[512,256]{1,0:T(8,128)(2,1)}), bf16[2048,256]{1,0:T(8,128)(2,1)}) %all-gather.29.cloned.1.call-update) | async-done | bytes 1048592 | tf_op jit(solution)/shard_map/all_gather | solution.py:95
  270.6 28.8 %all-gather.31.cloned.1.call-done = bf16[256,2048]{1,0:T(8,128)(2,1)} async-done(((bf16[256,512]{1,0:T(8,128)(2,1)}), bf16[256,2048]{1,0:T(8,128)(2,1)}) %all-gather.31.cloned.1.call-update) | async-done | bytes 1048592 | tf_op jit(solution)/shard_map/all_gather | solution.py:168
  300.0 6.5 %add_convert_fusion = bf16[512,2048]{1,0:T(8,128)(2,1)} fusion(f32[512,2048]{1,0:T(8,128)} %fusion.30, bf16[256,2048]{1,0:T(8,128)(2,1)} %all-gather.31.cloned.1.call-done, f32[64,8,2,128]{3,2,1,0:T(2,128)S(1)} %bitcast.95, f32[64,8,2,128]{3,2,1,0:T(2,128)S(1)} %bitcast.94, bf16[512,2048]{1,0:T(8,128)(2,1)S(1)} %copy-done, ...), kind=kOutput, calls=%fused_computation.6 | convolution fusion | flops 1077018624 | bytes 11534336 | tf_op jit(solution)/shard_map/dot_general | solution.py:173
  306.6 30.7 %reduce-scatter.2.cloned.1.call-done = bf16[128,2048]{1,0:T(8,128)(2,1)} async-done(((bf16[512,2048]{1,0:T(8,128)(2,1)}), bf16[128,2048]{1,0:T(8,128)(2,1)}) %reduce-scatter.2.cloned.1.call-update) | async-done | bytes 524304 | tf_op jit(solution)/shard_map/reduce_scatter | solution.py:170
  (90 shorter events, 12.9 us)
Async XLA Ops:
  6.5 33.4 %all-gather.25.cloned.1.call-start = ((), (), s32[]{:S(2)}) async-start(), calls=%async_computation.7 | async-start | bytes 1310720 | tf_op jit(solution)/shard_map/all_gather | solution.py:93
  7.3 56.2 %all-gather.13.cloned.1.call-start = ((), (), s32[]{:S(2)}) async-start(), calls=%async_computation.1 | async-start | bytes 2621440 | tf_op jit(solution)/shard_map/all_gather | solution.py:86
  8.0 8.7 %copy-start.14 = (f32[512,2]{0,1:T(2,128)S(1)}, f32[512,2]{0,1:T(2,128)}, u32[]{:S(2)}) copy-start(f32[512,2]{0,1:T(2,128)} %param.29) | copy-start | bytes 12292
  8.0 10.7 %copy-start.15 = (u32[32]{0:T(128)S(1)}, u32[32]{0:T(128)}, u32[]{:S(2)}) copy-start(u32[32]{0:T(128)} %constant.65) | copy-start | bytes 388
  8.0 28.8 %copy-start.10 = (bf16[3,256]{1,0:T(4,128)(2,1)S(1)}, bf16[3,256]{1,0:T(4,128)(2,1)}, u32[]{:S(2)}) copy-start(bf16[3,256]{1,0:T(4,128)(2,1)} %param.26) | copy-start | bytes 4612
  11.3 81.8 %all-gather.27.cloned.1.call-start = ((), (), s32[]{:S(2)}) async-start(), calls=%async_computation.8 | async-start | bytes 1310720 | tf_op jit(solution)/shard_map/all_gather | solution.py:92
  12.1 109.8 %all-gather.23.cloned.1.call-start = ((), (), s32[]{:S(2)}) async-start(), calls=%async_computation.6 | async-start | bytes 1310720 | tf_op jit(solution)/shard_map/all_gather | solution.py:94
  12.6 142.4 %all-gather.19.cloned.1.call-start = ((), (), s32[]{:S(2)}) async-start(), calls=%async_computation.4 | async-start | bytes 1310720 | tf_op jit(solution)/shard_map/all_gather | solution.py:91
  13.2 170.5 %all-gather.17.cloned.1.call-start = ((), (), s32[]{:S(2)}) async-start(), calls=%async_computation.3 | async-start | bytes 1310720 | tf_op jit(solution)/shard_map/all_gather | solution.py:90
  13.8 198.9 %all-gather.15.cloned.1.call-start = ((), (), s32[]{:S(2)}) async-start(), calls=%async_computation.2 | async-start | bytes 1310720 | tf_op jit(solution)/shard_map/all_gather | solution.py:89
  14.6 227.1 %all-gather.21.cloned.1.call-start = ((), (), s32[]{:S(2)}) async-start(), calls=%async_computation.5 | async-start | bytes 1310720 | tf_op jit(solution)/shard_map/all_gather | solution.py:167
  15.3 255.3 %all-gather.29.cloned.1.call-start = ((), (), s32[]{:S(2)}) async-start(), calls=%async_computation.9 | async-start | bytes 1310720 | tf_op jit(solution)/shard_map/all_gather | solution.py:95
  16.0 283.4 %all-gather.31.cloned.1.call-start = ((), (), s32[]{:S(2)}) async-start(), calls=%async_computation.10 | async-start | bytes 1310720 | tf_op jit(solution)/shard_map/all_gather | solution.py:168
  16.6 320.7 %reduce-scatter.2.cloned.1.call-start = ((), (), s32[]{:S(2)}) async-start(), calls=%async_computation.11 | async-start | bytes 2621440 | tf_op jit(solution)/shard_map/reduce_scatter | solution.py:170
  66.1 27.0 %copy-start = (bf16[512,2048]{1,0:T(8,128)(2,1)S(1)}, bf16[512,2048]{1,0:T(8,128)(2,1)}, u32[]{:S(2)}) copy-start(bf16[512,2048]{1,0:T(8,128)(2,1)} %all-gather.13.cloned.1.call-done) | copy-start | bytes 6291460
  123.9 2.9 copy-start.8
  183.7 6.7 %copy-start.3 = (f32[512,2,64]{2,0,1:T(8,128)S(1)}, f32[512,2,64]{2,0,1:T(8,128)}, u32[]{:S(2)}) copy-start(f32[512,2,64]{2,0,1:T(8,128)} %get-tuple-element.140) | copy-start | bytes 786436
  183.7 6.7 %copy-start.4 = (f32[512,2,64]{2,0,1:T(8,128)S(1)}, f32[512,2,64]{2,0,1:T(8,128)}, u32[]{:S(2)}) copy-start(f32[512,2,64]{2,0,1:T(8,128)} %get-tuple-element.141) | copy-start | bytes 786436
  183.7 6.9 %copy-start.6 = (f32[4,128,2]{1,2,0:T(2,128)S(1)}, f32[4,128,2]{1,2,0:T(2,128)}, u32[]{:S(2)}) copy-start(f32[4,128,2]{1,2,0:T(2,128)} %copy.73) | copy-start | bytes 12292
  185.9 4.5 %copy-start.1 = (f32[512,256]{1,0:T(8,128)}, f32[512,256]{1,0:T(8,128)S(1)}, u32[]{:S(2)}) copy-start(f32[512,256]{1,0:T(8,128)S(1)} %fusion.6) | copy-start | bytes 1572868
  186.6 55.1 %collective-permute-start = (f32[2,256]{1,0:T(2,128)}, f32[2,256]{1,0:T(2,128)}, u32[]{:S(2)}, u32[]{:S(2)}) collective-permute-start(f32[2,256]{1,0:T(2,128)} %slice.45), channel_id=1, source_target_pairs={{0,4},{4,8},{8,12},{1,5},{5,9},{9,13},{2,6},{6,10},{10,14},{3,7},{... | collective-permute-start | bytes 6152 | tf_op jit(solution)/shard_map/ppermute | solution.py:37
  190.6 1.8 copy-start.5
  190.7 1.8 copy-start.7
  190.7 1.8 copy-start.9
  192.4 49.2 %copy-start.2 = (f32[512,256]{1,0:T(8,128)S(1)}, f32[512,256]{1,0:T(8,128)}, u32[]{:S(2)}) copy-start(f32[512,256]{1,0:T(8,128)} %copy-done.1) | copy-start | bytes 1572868
  192.4 49.2 %copy-start.11 = (f32[1,256]{1,0:T(1,128)S(1)}, f32[1,256]{1,0:T(1,128)}, u32[]{:S(2)}) copy-start(f32[1,256]{1,0:T(1,128)} %get-tuple-element.154) | copy-start | bytes 3076
  192.4 49.2 %copy-start.12 = (f32[1,256]{1,0:T(1,128)S(1)}, f32[1,256]{1,0:T(1,128)}, u32[]{:S(2)}) copy-start(f32[1,256]{1,0:T(1,128)} %get-tuple-element.155) | copy-start | bytes 3076
  192.4 49.2 %copy-start.13 = (f32[1,256]{1,0:T(1,128)S(1)}, f32[1,256]{1,0:T(1,128)}, u32[]{:S(2)}) copy-start(f32[1,256]{1,0:T(1,128)} %get-tuple-element.156) | copy-start | bytes 3076
Sparse Core Ops, SparseCore 0:
  8.9 30.9 all-gather.24
  41.5 21.9 all-gather.12
  65.1 27.9 all-gather.26
  94.5 27.3 all-gather.22
  123.3 31.5 all-gather.18
  156.4 27.3 all-gather.16
  185.3 27.3 all-gather.14
  214.3 27.3 all-gather.20
  243.2 27.3 all-gather.28
  272.0 27.3 all-gather.30
  306.7 30.5 reduce-scatter.1
where the time goes:
time: 345 us; the launch traced here: 344 us
  waiting for transfers between devices  234 us (68%)
  blocking collectives  31.1 us (9%)
  matrix products  29.2 us (8%)
  other arithmetic  16 us (5%)
  local copies, waits for them, and re-layouts  15 us (4%)
  between operations  14.2 us (4%)
  starting transfers between devices  4.26 us (1%)
    reduce_scatter x1, waiting for transfers between devices, body(): lax.psum_scatter((jnp.dot(conv_branch, conv_rows_weight, preferred_elemen...  30.7 us
    all_gather x1, waiting for transfers between devices, body(): lax.all_gather(conv_out_weight, 'sp', axis=1, tiled=True)  29 us
    all_gather x1, waiting for transfers between devices, body(): lax.all_gather(ret_out_weight, 'sp', axis=1, tiled=True)  28.8 us
    all_gather x1, waiting for transfers between devices, body(): lax.all_gather(conv_inner_weight, 'sp', axis=0, tiled=True)  26 us
    all_gather x1, waiting for transfers between devices, body(): lax.all_gather(query_matrix, 'sp', axis=0, tiled=True)  24.9 us
    all_gather x1, waiting for transfers between devices, body(): lax.all_gather(value_weight, 'sp', axis=0, tiled=True)  24.8 us
    all_gather x1, waiting for transfers between devices, body(): gathered = lax.all_gather(normed, 'tp', axis=0, tiled=True)  23.6 us
    all_gather x1, waiting for transfers between devices, body(): lax.all_gather(gate_weight, 'sp', axis=0, tiled=True)  23.1 us
  transfers between devices with their start and end apart: 12, of which 10 were waited for; matrix products, arithmetic and copies ran while one was open for 15% of the time, Pallas kernels for 0%

commit v1 on v0

--- a/solution.py
+++ b/solution.py
@@ -165,7 +165,7 @@
     ).astype(jnp.bfloat16)
     conv_rows_weight, ret_rows_weight = (
         lax.all_gather(conv_out_weight, "sp", axis=1, tiled=True),
-        lax.all_gather(ret_out_weight, "sp", axis=1, tiled=True),
+        jnp.concatenate(lax.all_gather(ret_out_weight, "sp"), axis=1),
     )
     return lax.psum_scatter(
         (

time: 345 us -> 345 us (level)
    all_gather x1, waiting for transfers between devices: 28.8 us -> 0.74 us  [body(): lax.all_gather(ret_out_weight, 'sp')]
    all_gather x1, waiting for transfers between devices: 0.74 us -> 26.6 us  [body(): lax.all_gather(key_weight, 'sp', axis=0, tiled=True)]
  transfers between devices with their start and end apart: 12 -> 12, of which waited for: 10 -> 11; matrix products, arithmetic and copies ran while one was open for 15% -> 16% of each run, Pallas kernels for 0% -> 0%
where the time goes in v1:
time: 345 us
  waiting for transfers between devices  232 us (67%)
  blocking collectives  31.1 us (9%)
  matrix products  29.1 us (8%)
  local copies, waits for them, and re-layouts  17.8 us (5%)
  other arithmetic  15.9 us (5%)
  between operations  14.2 us (4%)
  starting transfers between devices  4.32 us (1%)
    reduce_scatter x1, waiting for transfers between devices, body(): lax.psum_scatter((jnp.dot(conv_branch, conv_rows_weight, preferred_elemen...  30.7 us
    all_gather x1, waiting for transfers between devices, body(): lax.all_gather(conv_out_weight, 'sp', axis=1, tiled=True)  29 us
    all_gather x1, waiting for transfers between devices, body(): lax.all_gather(key_weight, 'sp', axis=0, tiled=True)  26.6 us
    all_gather x1, waiting for transfers between devices, body(): lax.all_gather(conv_inner_weight, 'sp', axis=0, tiled=True)  26.1 us
    all_gather x1, waiting for transfers between devices, body(): lax.all_gather(value_weight, 'sp', axis=0, tiled=True)  24.8 us
    all_gather x1, waiting for transfers between devices, body(): lax.all_gather(query_matrix, 'sp', axis=0, tiled=True)  24.8 us
    all_gather x1, waiting for transfers between devices, body(): gathered = lax.all_gather(normed, 'tp', axis=0, tiled=True)  23.5 us
    all_gather x1, waiting for transfers between devices, body(): lax.all_gather(gate_weight, 'sp', axis=0, tiled=True)  22.3 us
  transfers between devices with their start and end apart: 12, of which 11 were waited for; matrix products, arithmetic and copies ran while one was open for 16% of the time, Pallas kernels for 0%

profile of v1, /device:TPU:0, one launch (start us, length us, event | category | flops | bytes accessed | tf_op | source)
XLA Modules:
  0.0 344.6 jit_solution(9947263242871581523)
XLA Ops:
  6.5 0.7 all-gather.32.cloned.1.call-update
  7.3 0.7 all-gather.26.cloned.1.call-update
  8.1 0.7 convert_element_type.96
  8.8 1.2 fusion.9
  10.0 2.0 fusion.11
  13.9 0.7 all-gather.18.cloned.1.call-update
  14.6 0.7 all-gather.16.cloned.1.call-update
  15.4 0.7 all-gather.22.cloned.1.call-update
  20.9 14.0 %all-reduce = bf16[8]{0:T(256)(128)(2,1)S(1)} all-reduce(bf16[8]{0:T(256)(128)(2,1)S(1)} %dynamic-update-slice), channel_id=2, replica_groups=mesh['grp'=2,'sp'=4,'tp'=4] {'sp'}, use_global_device_ids=true, to_apply=%add | all-reduce | flops 8 | bytes 32
  34.9 0.7 reshape.184
  37.4 1.8 multiply_cosine_fusion
  39.2 0.7 all-gather.32.cloned.1.call-done
  39.9 2.3 copy.112
  42.3 26.6 %all-gather.26.cloned.1.call-done = bf16[2048,256]{1,0:T(8,128)(2,1)} async-done(((bf16[512,256]{1,0:T(8,128)(2,1)}), bf16[2048,256]{1,0:T(8,128)(2,1)}) %all-gather.26.cloned.1.call-update) | async-done | bytes 1048592 | tf_op jit(solution)/shard_map/all_gather | solution.py:93
  68.9 23.5 %all-gather.14.cloned.1.call-done = bf16[512,2048]{1,0:T(8,128)(2,1)} async-done(((bf16[128,2048]{1,0:T(8,128)(2,1)}), bf16[512,2048]{1,0:T(8,128)(2,1)}) %all-gather.14.cloned.1.call-update) | async-done | bytes 2097168 | tf_op jit(solution)/shard_map/all_gather | solution.py:86
  92.4 2.6 convolution_convert_fusion.2
  95.1 1.0 copy.121
  96.1 1.0 copy.122
  97.1 24.8 %all-gather.28.cloned.1.call-done = bf16[2048,256]{1,0:T(8,128)(2,1)} async-done(((bf16[512,256]{1,0:T(8,128)(2,1)}), bf16[2048,256]{1,0:T(8,128)(2,1)}) %all-gather.28.cloned.1.call-update) | async-done | bytes 1048592 | tf_op jit(solution)/shard_map/all_gather | solution.py:92
  121.8 2.0 convolution_convert_fusion.1
  123.9 1.0 copy.123
  124.9 1.0 copy.124
  125.9 24.8 %all-gather.24.cloned.1.call-done = bf16[2048,256]{1,0:T(8,128)(2,1)} async-done(((bf16[512,256]{1,0:T(8,128)(2,1)}), bf16[2048,256]{1,0:T(8,128)(2,1)}) %all-gather.24.cloned.1.call-update) | async-done | bytes 1048592 | tf_op jit(solution)/shard_map/all_gather | solution.py:94
  150.6 1.9 convolution_convert_fusion.3
  152.7 2.9 multiply_subtract_fusion
  155.5 1.7 fusion.23
  157.2 9.3 %while.26 = (s32[]{:T(128)}, f32[2,128,128]{2,1,0:T(8,128)S(1)}, f32[4,2,128,128]{3,2,1,0:T(8,128)}, f32[4,2]{1,0:T(4,128)}, f32[4,2,128,128]{3,2,1,0:T(8,128)}, /*index=5*/s32[]{:T(128)}, s32[]{:T(128)}) while((s32[]{:T(128)}, f32[2,128,128]{2,1,0:T(8,128)S(1)}, f32[4,2,128,128]{3,2,1,0:T(8,128)}, f32[4,2]{1,0:T(4,128)}, ...), condition=%wide.region_2.3_spmd.clone, body=%wide.region_1.2_spmd.clone.sunk | while | flops 131075 | bytes 655992 | solution.py:140
  158.5 1.0 bitcast_add_fusion.2
  159.5 0.7 bitcast_dynamic-update-slice_fusion.2
  160.9 1.0 bitcast_add_fusion.2
  161.9 0.7 bitcast_dynamic-update-slice_fusion.2
  163.2 1.0 bitcast_add_fusion.2
  165.5 1.0 bitcast_add_fusion.2
  166.5 17.1 %all-gather.1 = bf16[8,128,128]{2,1,0:T(8,128)(2,1)} all-gather(bf16[2,128,128]{2,1,0:T(8,128)(2,1)S(1)} %convert_element_type.112), channel_id=3, replica_groups=mesh['grp'=2,'sp'=4,'tp'=4] {'sp'}, dimensions={0}, use_global_device_ids=true | all-gather | bytes 327680 | tf_op jit(solution)/shard_map/all_gather | solution.py:17
  183.8 2.7 fusion.7
  186.5 26.1 %all-gather.18.cloned.1.call-done = bf16[2048,256]{1,0:T(8,128)(2,1)} async-done(((bf16[512,256]{1,0:T(8,128)(2,1)}), bf16[2048,256]{1,0:T(8,128)(2,1)}) %all-gather.18.cloned.1.call-update) | async-done | bytes 1048592 | tf_op jit(solution)/shard_map/all_gather | solution.py:90
  212.6 2.2 fusion.6
  215.4 3.9 %collective-permute-start = (f32[2,256]{1,0:T(2,128)}, f32[2,256]{1,0:T(2,128)}, u32[]{:S(2)}, u32[]{:S(2)}) collective-permute-start(f32[2,256]{1,0:T(2,128)} %slice.45), channel_id=1, source_target_pairs={{0,4},{4,8},{8,12},{1,5},{5,9},{9,13},{2,6},{6,10},{10,14},{3,7},{... | collective-permute-start | bytes 6152 | tf_op jit(solution)/shard_map/ppermute | solution.py:37
  219.6 1.3 fusion.3
  221.4 1.1 multiply_reduce_fusion
  222.7 1.1 copy.110
  223.8 17.8 %all-gather.16.cloned.1.call-done = bf16[2048,256]{1,0:T(8,128)(2,1)} async-done(((bf16[512,256]{1,0:T(8,128)(2,1)}), bf16[2048,256]{1,0:T(8,128)(2,1)}) %all-gather.16.cloned.1.call-update) | async-done | bytes 1048592 | tf_op jit(solution)/shard_map/all_gather | solution.py:89
  241.6 29.0 %all-gather.22.cloned.1.call-done = bf16[256,2048]{1,0:T(8,128)(2,1)} async-done(((bf16[256,512]{1,0:T(8,128)(2,1)}), bf16[256,2048]{1,0:T(8,128)(2,1)}) %all-gather.22.cloned.1.call-update) | async-done | bytes 1048592 | tf_op jit(solution)/shard_map/all_gather | solution.py:167
  270.6 6.5 %fusion.30 = f32[512,2048]{1,0:T(8,128)} fusion(bf16[256,2048]{1,0:T(8,128)(2,1)} %all-gather.22.cloned.1.call-done, f32[2,256]{1,0:T(2,128)} %collective-permute-done, f32[512,256]{1,0:T(8,128)} %copy-done.2, bf16[512,2048]{1,0:T(8,128)(2,1)S(1)} %copy-done, bf16[2048,256]{1,0:T(8,128)(2,1)} %all-gather.16.cloned.1.call-done, f32[256]{0:T(256)S(1)} %bitcast.107, ...), kind=kOutput, calls=%fused_computation.62 | convolution fusion | flops 1075183616 | bytes 8918016 | tf_op jit(solution)/shard_map/dot_general | solution.py:172
  277.1 22.3 %all-gather.30.cloned.1.call-done = bf16[2048,256]{1,0:T(8,128)(2,1)} async-done(((bf16[512,256]{1,0:T(8,128)(2,1)}), bf16[2048,256]{1,0:T(8,128)(2,1)}) %all-gather.30.cloned.1.call-update) | async-done | bytes 1048592 | tf_op jit(solution)/shard_map/all_gather | solution.py:95
  299.4 1.4 mul.252
  300.8 6.5 %add_convert_fusion = bf16[512,2048]{1,0:T(8,128)(2,1)} fusion(f32[512,2048]{1,0:T(8,128)} %fusion.30, bf16[256,2048]{0,1:T(8,128)(2,1)S(1)} %bitcast.98, f32[64,8,2,128]{3,2,1,0:T(2,128)} %bitcast.100, f32[64,8,2,128]{3,2,1,0:T(2,128)} %bitcast.99, bf16[512,2048]{1,0:T(8,128)(2,1)S(1)} %copy-done, bf16[2048,256]{1,0:T(8,128)(2,1)} %all-gather.30.cloned.1.call-done), kind=kOutput, calls=%fused_computation.6 | convolution fusion | flops 1077018624 | bytes 11534336 | tf_op jit(solution)/shard_map/dot_general | solution.py:173
  307.3 30.7 %reduce-scatter.2.cloned.1.call-done = bf16[128,2048]{1,0:T(8,128)(2,1)} async-done(((bf16[512,2048]{1,0:T(8,128)(2,1)}), bf16[128,2048]{1,0:T(8,128)(2,1)}) %reduce-scatter.2.cloned.1.call-update) | async-done | bytes 524304 | tf_op jit(solution)/shard_map/reduce_scatter | solution.py:170
  (91 shorter events, 13.7 us)
Async XLA Ops:
  6.5 33.4 %all-gather.32.cloned.1.call-start = ((), (), s32[]{:S(2)}) async-start(), calls=%async_computation.11 | async-start | bytes 1310720 | tf_op jit(solution)/shard_map/all_gather | solution.py:168
  7.3 9.5 %copy-start.14 = (f32[512,2]{0,1:T(2,128)S(1)}, f32[512,2]{0,1:T(2,128)}, u32[]{:S(2)}) copy-start(f32[512,2]{0,1:T(2,128)} %param.29) | copy-start | bytes 12292
  7.3 61.6 %all-gather.26.cloned.1.call-start = ((), (), s32[]{:S(2)}) async-start(), calls=%async_computation.7 | async-start | bytes 1310720 | tf_op jit(solution)/shard_map/all_gather | solution.py:93
  8.0 10.7 %copy-start.15 = (u32[32]{0:T(128)S(1)}, u32[32]{0:T(128)}, u32[]{:S(2)}) copy-start(u32[32]{0:T(128)} %constant.65) | copy-start | bytes 388
  8.0 28.8 %copy-start.10 = (bf16[3,256]{1,0:T(4,128)(2,1)S(1)}, bf16[3,256]{1,0:T(4,128)(2,1)}, u32[]{:S(2)}) copy-start(bf16[3,256]{1,0:T(4,128)(2,1)} %param.26) | copy-start | bytes 4612
  8.0 84.4 %all-gather.14.cloned.1.call-start = ((), (), s32[]{:S(2)}) async-start(), calls=%async_computation.1 | async-start | bytes 2621440 | tf_op jit(solution)/shard_map/all_gather | solution.py:86
  12.1 109.8 %all-gather.28.cloned.1.call-start = ((), (), s32[]{:S(2)}) async-start(), calls=%async_computation.8 | async-start | bytes 1310720 | tf_op jit(solution)/shard_map/all_gather | solution.py:92
  12.6 138.0 %all-gather.24.cloned.1.call-start = ((), (), s32[]{:S(2)}) async-start(), calls=%async_computation.6 | async-start | bytes 1310720 | tf_op jit(solution)/shard_map/all_gather | solution.py:94
  13.2 170.5 %all-gather.20.cloned.1.call-start = ((), (), s32[]{:S(2)}) async-start(), calls=%async_computation.4 | async-start | bytes 1310720 | tf_op jit(solution)/shard_map/all_gather | solution.py:91
  13.8 198.8 %all-gather.18.cloned.1.call-start = ((), (), s32[]{:S(2)}) async-start(), calls=%async_computation.3 | async-start | bytes 1310720 | tf_op jit(solution)/shard_map/all_gather | solution.py:90
  14.6 227.0 %all-gather.16.cloned.1.call-start = ((), (), s32[]{:S(2)}) async-start(), calls=%async_computation.2 | async-start | bytes 1310720 | tf_op jit(solution)/shard_map/all_gather | solution.py:89
  15.3 255.3 %all-gather.22.cloned.1.call-start = ((), (), s32[]{:S(2)}) async-start(), calls=%async_computation.5 | async-start | bytes 1310720 | tf_op jit(solution)/shard_map/all_gather | solution.py:167
  16.0 283.3 %all-gather.30.cloned.1.call-start = ((), (), s32[]{:S(2)}) async-start(), calls=%async_computation.9 | async-start | bytes 1310720 | tf_op jit(solution)/shard_map/all_gather | solution.py:95
  16.6 321.4 %reduce-scatter.2.cloned.1.call-start = ((), (), s32[]{:S(2)}) async-start(), calls=%async_computation.10 | async-start | bytes 2621440 | tf_op jit(solution)/shard_map/reduce_scatter | solution.py:170
  95.0 26.8 %copy-start = (bf16[512,2048]{1,0:T(8,128)(2,1)S(1)}, bf16[512,2048]{1,0:T(8,128)(2,1)}, u32[]{:S(2)}) copy-start(bf16[512,2048]{1,0:T(8,128)(2,1)} %all-gather.14.cloned.1.call-done) | copy-start | bytes 6291460
  152.7 2.9 copy-start.8
  212.6 6.8 %copy-start.3 = (f32[512,2,64]{2,0,1:T(8,128)S(1)}, f32[512,2,64]{2,0,1:T(8,128)}, u32[]{:S(2)}) copy-start(f32[512,2,64]{2,0,1:T(8,128)} %get-tuple-element.145) | copy-start | bytes 786436
  212.6 6.8 %copy-start.4 = (f32[512,2,64]{2,0,1:T(8,128)S(1)}, f32[512,2,64]{2,0,1:T(8,128)}, u32[]{:S(2)}) copy-start(f32[512,2,64]{2,0,1:T(8,128)} %get-tuple-element.146) | copy-start | bytes 786436
  212.6 7.0 %copy-start.6 = (f32[4,128,2]{1,2,0:T(2,128)S(1)}, f32[4,128,2]{1,2,0:T(2,128)}, u32[]{:S(2)}) copy-start(f32[4,128,2]{1,2,0:T(2,128)} %copy.98) | copy-start | bytes 12292
  214.8 4.6 %copy-start.2 = (f32[512,256]{1,0:T(8,128)}, f32[512,256]{1,0:T(8,128)S(1)}, u32[]{:S(2)}) copy-start(f32[512,256]{1,0:T(8,128)S(1)} %fusion.6) | copy-start | bytes 1572868
  215.4 55.1 %collective-permute-start = (f32[2,256]{1,0:T(2,128)}, f32[2,256]{1,0:T(2,128)}, u32[]{:S(2)}, u32[]{:S(2)}) collective-permute-start(f32[2,256]{1,0:T(2,128)} %slice.45), channel_id=1, source_target_pairs={{0,4},{4,8},{8,12},{1,5},{5,9},{9,13},{2,6},{6,10},{10,14},{3,7},{... | collective-permute-start | bytes 6152 | tf_op jit(solution)/shard_map/ppermute | solution.py:37
  219.6 1.8 copy-start.5
  219.6 1.8 copy-start.7
  219.6 1.8 copy-start.9
  221.4 49.2 %copy-start.11 = (f32[1,256]{1,0:T(1,128)S(1)}, f32[1,256]{1,0:T(1,128)}, u32[]{:S(2)}) copy-start(f32[1,256]{1,0:T(1,128)} %get-tuple-element.159) | copy-start | bytes 3076
  221.4 49.2 %copy-start.12 = (f32[1,256]{1,0:T(1,128)S(1)}, f32[1,256]{1,0:T(1,128)}, u32[]{:S(2)}) copy-start(f32[1,256]{1,0:T(1,128)} %get-tuple-element.160) | copy-start | bytes 3076
  221.4 49.2 %copy-start.13 = (f32[1,256]{1,0:T(1,128)S(1)}, f32[1,256]{1,0:T(1,128)}, u32[]{:S(2)}) copy-start(f32[1,256]{1,0:T(1,128)} %get-tuple-element.161) | copy-start | bytes 3076
  270.6 30.2 %copy-start.1 = (bf16[256,4,512]{0,2,1:T(8,128)(2,1)S(1)}, bf16[256,4,512]{0,2,1:T(8,128)(2,1)}, u32[]{:S(2)}) copy-start(bf16[256,4,512]{0,2,1:T(8,128)(2,1)} %copy.112) | copy-start | bytes 3145732
Sparse Core Ops, SparseCore 0:
  8.9 30.9 all-gather.31
  41.5 27.3 all-gather.25
  70.4 21.9 all-gather.13
  93.8 27.9 all-gather.27
  123.3 27.3 all-gather.23
  152.1 31.6 all-gather.19
  185.3 27.2 all-gather.17
  214.2 27.3 all-gather.15
  243.2 27.3 all-gather.21
  272.0 27.3 all-gather.29
  307.5 30.5 reduce-scatter.1
